TPU v7x, 32 devices: a whole 2x2x4 slice. The times are simulated.
32 devices in a mesh: sp: 8 (over z, x), tp: 4 (over y, core).
Axes of the slice: x: 2, y: 2, z: 4, core: 2. Of those that a mesh axis runs over, the one named last changes fastest.
Arguments:
- conv_gate: bfloat16 [2048, 512], P('sp', 'tp'), may hold values from -6 to 6
- conv_mix: bfloat16 [2048, 512], P('sp', 'tp'), may hold values from -6 to 6
- conv_input: bfloat16 [2048, 512], P('sp', 'tp'), may hold values from -6 to 6
- conv_taps: bfloat16 [3, 512], P(None, 'tp'), may hold values from -3.5 to 3.5
- query_rows: bfloat16 [2048, 512], P('sp', 'tp'), may hold values from -50 to 50, as said below
- key_rows: bfloat16 [2048, 512], P('sp', 'tp'), may hold values from -10 to 10, as said below
- value_rows: bfloat16 [2048, 512], P('sp', 'tp'), may hold values from -6 to 6
- lambdas: float32 [4], P('tp'), may hold values from 0.3 to 0.8
- head_gain: float32 [128], replicated, may hold values from 0.1 to 1.9
- w_out_conv: bfloat16 [512, 2048], P('tp'), may hold values from -0.1875 to 0.1875
- w_out_heads: bfloat16 [512, 2048], P('tp'), may hold values from -0.1875 to 0.1875
Outputs:
- mixed: bfloat16 [2048, 2048], P(('sp', 'tp'))
Inputs may be any that keep to these rules, and one draw needn't show every extreme that they name: `query_rows`: queries of order one; some rows may be far larger. `key_rows`: keys of order one.
All inputs are finite; a program needn't handle non-finite values.
Results may differ from a plain program's by a relative error of at most 0.013.
Values may be sent and summed in bfloat16 or wider, within the bound.
A program may use at most 128 MiB of HBM per device.

v0:
```python
import functools

import jax
import jax.numpy as jnp
from jax import lax
from jax.experimental import pallas as pl
from jax.experimental.pallas import tpu as pltpu
from jax.sharding import PartitionSpec as P

HEAD_QK = 64
PIECES = 2
COL_TILE = 512
LATE_TILES = 1
MESH = pl.DeviceIdType.MESH
F32 = jnp.float32
BF16 = jnp.bfloat16


def kernel(
    n_sp,
    n_tp,
    gate_h,
    mix_h,
    inp_h,
    taps_h,
    q_h,
    k_h,
    v_h,
    lam_ref,
    gain_h,
    wc_h,
    wh_h,
    out_ref,
    gate,
    mix,
    inp,
    taps,
    gain,
    q,
    col,
    cross,
    halo,
    ext,
    conv,
    wc,
    wh,
    cxs,
    cxr,
    cys,
    cyr,
    own,
    fxs,
    fxr,
    head,
    hact,
    pys,
    pyr,
    peak,
    denom,
    acc,
    load_sem,
    halo_ss,
    halo_rs,
    up_ss,
    col_rs,
    x_ss,
    cross_rs,
    w_ss,
    w_rs,
    cx_ss,
    cx_rs,
    cy_ss,
    cy_rs,
    ha_ss,
    ha_rs,
    fx_ss,
    fx_rs,
    py_ss,
    py_rs,
):
    s = lax.axis_index("sp")
    t = lax.axis_index("tp")
    levels, outer = n_sp // 2, n_tp // 2
    z, x = s // 2, s % 2
    a, b = t // 2, t % 2
    rows = q.shape[0]
    width = out_ref.shape[1]
    chunk = rows // n_tp
    piece = rows // PIECES
    has_next = s < n_sp - 1
    has_prev = s > 0
    has_up = z < levels - 1
    has_down = z > 0

    def at(sp, tp):
        return {"device_id": (sp, tp), "device_id_type": MESH}

    barrier = pltpu.get_barrier_semaphore()
    ups, downs, side = (z + 1) * 2 + x, (z - 1) * 2 + x, z * 2 + 1 - x

    def greet(sp, tp):
        pl.semaphore_signal(barrier, inc=1, **at(sp, tp))

    pl.when(has_next)(lambda: greet(s + 1, t))
    pl.when(has_prev)(lambda: greet(s - 1, t))
    pl.when(has_up)(lambda: greet(ups, t))
    pl.when(has_down)(lambda: greet(downs, t))
    greet(side, t)
    for step in range(1, n_tp):
        greet(s, lax.rem(t + step, n_tp))

    loads = [
        pltpu.make_async_copy(source, target, load_sem.at[index])
        for index, (source, target) in enumerate(
            [
                (k_h.at[pl.ds(p * piece, piece)], col.at[z, 0, pl.ds(p * piece, piece)])
                for p in range(PIECES)
            ]
            + [
                (v_h.at[pl.ds(p * piece, piece)], col.at[z, 1, pl.ds(p * piece, piece)])
                for p in range(PIECES)
            ]
            + [
                (q_h, q),
                (mix_h, mix),
                (inp_h, inp),
                (gate_h, gate),
                (taps_h, taps),
                (gain_h, gain),
                (wc_h, wc),
                (wh_h, wh.at[pl.ds(a * wh_h.shape[0], wh_h.shape[0])]),
            ]
        )
    ]
    for load in loads:
        load.start()
    own_kv, (ld_q, ld_mix, ld_inp, ld_gate, ld_taps, ld_gain, ld_wc, ld_wh) = (
        loads[: 2 * PIECES],
        loads[2 * PIECES :],
    )

    pl.semaphore_wait(
        barrier,
        n_tp
        + has_next.astype(jnp.int32)
        + has_prev.astype(jnp.int32)
        + has_up.astype(jnp.int32)
        + has_down.astype(jnp.int32),
    )

    def part(blocks, level, p):
        return blocks.at[level, :, pl.ds(p * piece, piece), :]

    def up_copy(level, p):
        return pltpu.make_async_remote_copy(
            part(col, level, p), part(col, level, p), up_ss.at[level, p], col_rs.at[level, p], **at(ups, t)
        )

    def x_copy(level, p):
        return pltpu.make_async_remote_copy(
            part(col, level, p), part(cross, level, p), x_ss.at[level, p], cross_rs.at[level, p], **at(side, t)
        )

    def halo_copy(source, slot):
        return pltpu.make_async_remote_copy(
            source.at[pl.ds(rows - 16, 16)], halo.at[slot], halo_ss.at[slot], halo_rs.at[slot], **at(s + 1, t)
        )

    def forward(level, p, across=True):
        pl.when(has_up)(lambda: up_copy(level, p).start())
        if across is True:
            x_copy(level, p).start()
        else:
            pl.when(across)(lambda: x_copy(level, p).start())

    for p in range(PIECES):
        own_kv[p].wait()
        own_kv[PIECES + p].wait()
        forward(z, p, x == 0)

    ld_mix.wait()
    ld_inp.wait()

    @pl.when(has_next)
    def _():
        halo_copy(mix, 0).start()
        halo_copy(inp, 1).start()

    depth = wh_h.shape[0]
    late = LATE_TILES * COL_TILE
    early = width - late

    def w_copy(step):
        other = lax.rem(a + step, outer)
        mine = pl.ds(a * depth, depth)
        return pltpu.make_async_remote_copy(
            wh.at[mine, pl.ds(0, early)], wh.at[mine, pl.ds(0, early)], w_ss.at[step - 1], w_rs.at[step - 1], **at(s, other * 2 + b)
        )

    ld_wh.wait()
    for step in range(1, outer):
        w_copy(step).start()

    ld_q.wait()
    scale = HEAD_QK ** (-0.5)
    q[...] = (q[...].astype(F32) * scale).astype(BF16)

    def scores_of(block, m):
        lanes = slice(m * HEAD_QK, (m + 1) * HEAD_QK)
        return lax.dot_general(
            q[:, lanes], block[0, :, lanes], (((1,), (1,)), ((), ())), preferred_element_type=F32
        )

    ones = jnp.ones((rows, depth), BF16)

    def attend(block, first):
        tops, scored = [], []
        for m in range(2):
            scores = scores_of(block, m)
            if first:
                ahead = lax.broadcasted_iota(jnp.int32, scores.shape, 0)
                keys = lax.broadcasted_iota(jnp.int32, scores.shape, 1)
                scores = jnp.where(keys <= ahead, scores, -jnp.inf)
            top = jnp.max(scores, axis=1, keepdims=True)
            scored.append(scores)
            tops.append(top)
        for m in range(2):
            top = jnp.broadcast_to(tops[m], (rows, depth))
            if not first:
                before = peak[m]
                top = jnp.maximum(before, top)
                shrink = jnp.exp(before - top)
            wide = jnp.concatenate([top] * (rows // depth), axis=1) if rows > depth else top
            weights = jnp.exp(scored[m] - wide).astype(BF16)
            total = jnp.dot(weights, ones, preferred_element_type=F32)
            numer = jnp.dot(weights, block[1], preferred_element_type=F32)
            if not first:
                total = total + denom[m] * shrink
                numer = numer + acc[m] * shrink
            peak[m] = top
            denom[m] = total
            acc[m] = numer

    def attend_two(left, right):
        scored = [[scores_of(block, m) for block in (left, right)] for m in range(2)]
        tops = [
            jnp.max(jnp.maximum(scored[m][0], scored[m][1]), axis=1, keepdims=True) for m in range(2)
        ]
        for m in range(2):
            before = peak[m]
            top = jnp.maximum(before, jnp.broadcast_to(tops[m], (rows, depth)))
            shrink = jnp.exp(before - top)
            wide = jnp.concatenate([top] * (rows // depth), axis=1) if rows > depth else top
            total = denom[m] * shrink
            numer = acc[m] * shrink
            for scores, block in zip(scored[m], (left, right)):
                weights = jnp.exp(scores - wide).astype(BF16)
                total = total + jnp.dot(weights, ones, preferred_element_type=F32)
                numer = numer + jnp.dot(weights, block[1], preferred_element_type=F32)
            peak[m] = top
            denom[m] = total
            acc[m] = numer

    attend(col.at[z], True)

    ld_gate.wait()
    ld_taps.wait()
    ld_gain.wait()

    def gated(u, v):
        return (u.astype(F32) * v.astype(F32)).astype(BF16).astype(F32)

    ext[pl.ds(8, rows), :] = gated(mix[...], inp[...])

    @pl.when(has_prev)
    def _():
        halo_copy(mix, 0).wait_recv()
        halo_copy(inp, 1).wait_recv()
        ext[pl.ds(0, 8), :] = gated(halo[0], halo[1])[8:16]

    @pl.when(jnp.logical_not(has_prev))
    def _():
        ext[pl.ds(0, 8), :] = jnp.zeros((8, ext.shape[1]), F32)

    taps_v = taps[...].astype(F32)
    conv[...] = (
        gate[...].astype(F32)
        * (
            taps_v[0:1] * ext[pl.ds(6, rows), :]
            + taps_v[1:2] * ext[pl.ds(7, rows), :]
            + taps_v[2:3] * ext[pl.ds(8, rows), :]
        )
    ).astype(BF16)

    ld_wc.wait()
    partner = a * 2 + 1 - b

    def rows_of(oa, ob):
        return pl.ds(pl.multiple_of((oa * 2 + ob) * chunk, chunk), chunk)

    tiles = [slice(c, c + COL_TILE) for c in range(0, width, COL_TILE)]
    early_tiles, late_tiles = tiles[:-LATE_TILES], tiles[-LATE_TILES:]

    def cx_copy(step):
        return pltpu.make_async_remote_copy(
            cxs.at[step - 1], cxr.at[step - 1], cx_ss.at[step - 1], cx_rs.at[step - 1], **at(s, partner)
        )

    def cy_copy(step):
        other = lax.rem(a + step, outer)
        return pltpu.make_async_remote_copy(
            cys.at[step - 1], cyr.at[step - 1], cy_ss.at[step - 1], cy_rs.at[step - 1], **at(s, other * 2 + b)
        )

    for step in range(1, outer):
        other = lax.rem(a + step, outer)
        for tile in early_tiles:
            cxs[step - 1, :, tile] = jnp.dot(
                conv[rows_of(other, 1 - b), :], wc[:, tile], preferred_element_type=F32
            ).astype(BF16)
        cx_copy(step).start()

    def send_conv():
        for step in range(1, outer):
            other = lax.rem(a + step, outer)
            cx_copy(step).wait_recv()
            for tile in early_tiles:
                cys[step - 1, :, tile] = (
                    jnp.dot(conv[rows_of(other, b), :], wc[:, tile], preferred_element_type=F32)
                    + cxr[step - 1, :, tile].astype(F32)
                ).astype(BF16)
            cy_copy(step).start()

    pl.when(z == 0)(send_conv)

    def take_cross(level):
        for p in range(PIECES):
            x_copy(level, p).wait_recv()
        attend(cross.at[level], False)

    def advance(k, carry):
        level = z - k
        for p in range(PIECES):
            up_copy(level, p).wait_recv()
            forward(level, p)
        pl.when(k == 1)(send_conv)

        @pl.when(jnp.logical_or(k > 1, x == 1))
        def _():
            for p in range(PIECES):
                x_copy(level + 1, p).wait_recv()
            attend_two(cross.at[level + 1], col.at[level])

        pl.when(jnp.logical_and(k == 1, x == 0))(lambda: attend(col.at[level], False))
        return carry

    lax.fori_loop(1, z + 1, advance, 0)
    pl.when(jnp.logical_or(z > 0, x == 1))(lambda: take_cross(0))

    def merge(oa):
        chosen = pl.ds(pl.multiple_of(oa * 2 * chunk, 2 * chunk), 2 * chunk)
        merged = acc[0, chosen, :] / denom[0, chosen, :] - lam_ref[0] * (
            acc[1, chosen, :] / denom[1, chosen, :]
        )
        norm = lax.rsqrt(jnp.mean(merged * merged, axis=1, keepdims=True) + 1e-06)
        head[chosen, :] = (merged * norm * gain[...] * 0.8).astype(BF16)

    def ha_copy(step):
        other = lax.rem(a + step, outer)
        lanes = pl.ds(pl.multiple_of(a * depth, depth), depth)
        return pltpu.make_async_remote_copy(
            head.at[pl.ds(pl.multiple_of(other * 2 * chunk, 2 * chunk), 2 * chunk)],
            hact.at[:, lanes],
            ha_ss.at[step - 1],
            ha_rs.at[step - 1],
            **at(s, other * 2 + b),
        )

    for step in range(1, outer):
        merge(lax.rem(a + step, outer))
        ha_copy(step).start()
    merge(a)
    hact[:, pl.ds(pl.multiple_of(a * depth, depth), depth)] = head[
        pl.ds(pl.multiple_of(a * 2 * chunk, 2 * chunk), 2 * chunk), :
    ]
    held = pl.ds(pl.multiple_of(a * depth, depth), depth)

    def py_copy(step, ob):
        other = lax.rem(a + step, outer)
        return pltpu.make_async_remote_copy(
            pys.at[step - 1, ob],
            pyr.at[step - 1, b],
            py_ss.at[step - 1, ob],
            py_rs.at[step - 1, b],
            **at(s, other * 2 + ob),
        )

    def py_arrival(step, ob):
        return pltpu.make_async_remote_copy(
            pys.at[step - 1, ob],
            pyr.at[step - 1, ob],
            py_ss.at[step - 1, ob],
            py_rs.at[step - 1, ob],
            **at(s, lax.rem(a + step, outer) * 2 + ob),
        )

    def local(chosen, tile):
        return jnp.dot(conv[chosen, :], wc[:, tile], preferred_element_type=F32) + jnp.dot(
            head[chosen, :], wh[held, tile], preferred_element_type=F32
        )

    for step in range(1, outer):
        other = lax.rem(a + step, outer)
        for ob in range(2):
            for index, tile in enumerate(late_tiles):
                pys[step - 1, ob, :, index * COL_TILE : (index + 1) * COL_TILE] = local(
                    rows_of(other, ob), tile
                ).astype(BF16)
            py_copy(step, ob).start()
    for step in range(1, outer):
        w_copy(step).wait_recv()
    for step in range(1, outer):
        ha_copy(step).wait_recv()

    def fx_copy(index):
        lanes = tiles[index]
        return pltpu.make_async_remote_copy(
            fxs.at[:, lanes], fxr.at[:, lanes], fx_ss.at[index], fx_rs.at[index], **at(s, partner)
        )

    def contribution(ob, tile):
        mine = pl.ds(pl.multiple_of(ob * chunk, chunk), chunk)
        return jnp.dot(conv[rows_of(a, ob), :], wc[:, tile], preferred_element_type=F32) + jnp.dot(
            hact[mine, :], wh[:, tile], preferred_element_type=F32
        )

    def owed(ob, index):
        tile = tiles[index]
        return local(rows_of(a, ob), tile) if tile in late_tiles else contribution(ob, tile)

    order = list(range(len(early_tiles), len(tiles))) + list(range(len(early_tiles)))
    for index in order:
        fxs[:, tiles[index]] = owed(1 - b, index).astype(BF16)
        fx_copy(index).start()
    for step in range(1, outer):
        cy_copy(step).wait_recv()
    for index in order:
        tile = tiles[index]
        total = owed(b, index)
        if tile in early_tiles:
            for step in range(1, outer):
                total = total + cyr[step - 1, :, tile].astype(F32)
        own[:, tile] = total
    for step in range(1, outer):
        for ob in range(2):
            py_arrival(step, ob).wait_recv()
    for index in order:
        tile = tiles[index]
        total = own[:, tile]
        if tile in late_tiles:
            at_late = (index - len(early_tiles)) * COL_TILE
            for step in range(1, outer):
                for ob in range(2):
                    total = total + pyr[step - 1, ob, :, at_late : at_late + COL_TILE].astype(F32)
        fx_copy(index).wait_recv()
        out_ref[:, tile] = (total + fxr[:, tile].astype(F32)).astype(out_ref.dtype)

    def drain(level, carry):
        for p in range(PIECES):
            pl.when(has_up)(lambda: up_copy(level, p).wait_send())
            pl.when(jnp.logical_or(level < z, x == 0))(lambda: x_copy(level, p).wait_send())
        return carry

    lax.fori_loop(0, z + 1, drain, 0)

    @pl.when(has_next)
    def _():
        halo_copy(mix, 0).wait_send()
        halo_copy(inp, 1).wait_send()

    for step in range(1, outer):
        w_copy(step).wait_send()
        cx_copy(step).wait_send()
        cy_copy(step).wait_send()
        ha_copy(step).wait_send()
        for ob in range(2):
            py_copy(step, ob).wait_send()
    for index in range(len(tiles)):
        fx_copy(index).wait_send()


def shards(n_sp, n_tp, *args):
    gate, mix, inp, taps, q, k, v, lam, gain, wc, wh = args
    rows, lanes = q.shape
    depth, width = wh.shape
    levels, outer = n_sp // 2, n_tp // 2
    chunk = rows // n_tp
    tiles = width // COL_TILE
    late = LATE_TILES * COL_TILE
    dma = pltpu.SemaphoreType.DMA
    hbm = pl.BlockSpec(memory_space=pltpu.HBM)
    scratch = [
        pltpu.VMEM(gate.shape, BF16),
        pltpu.VMEM(mix.shape, BF16),
        pltpu.VMEM(inp.shape, BF16),
        pltpu.VMEM(taps.shape, BF16),
        pltpu.VMEM((1, gain.shape[0]), F32),
        pltpu.VMEM(q.shape, BF16),
        pltpu.VMEM((levels, 2, rows, lanes), BF16),
        pltpu.VMEM((levels, 2, rows, lanes), BF16),
        pltpu.VMEM((2, 16, mix.shape[1]), BF16),
        pltpu.VMEM((rows + 8, mix.shape[1]), F32),
        pltpu.VMEM(gate.shape, BF16),
        pltpu.VMEM(wc.shape, BF16),
        pltpu.VMEM((outer * depth, width), BF16),
        pltpu.VMEM((outer - 1, chunk, width - late), BF16),
        pltpu.VMEM((outer - 1, chunk, width - late), BF16),
        pltpu.VMEM((outer - 1, chunk, width - late), BF16),
        pltpu.VMEM((outer - 1, chunk, width - late), BF16),
        pltpu.VMEM((chunk, width), F32),
        pltpu.VMEM((chunk, width), BF16),
        pltpu.VMEM((chunk, width), BF16),
        pltpu.VMEM((rows, depth), BF16),
        pltpu.VMEM((2 * chunk, outer * depth), BF16),
        pltpu.VMEM((outer - 1, 2, chunk, late), BF16),
        pltpu.VMEM((outer - 1, 2, chunk, late), BF16),
        pltpu.VMEM((2, rows, depth), F32),
        pltpu.VMEM((2, rows, depth), F32),
        pltpu.VMEM((2, rows, depth), F32),
        dma((2 * PIECES + 8,)),
        dma((2,)),
        dma((2,)),
        dma((levels, PIECES)),
        dma((levels, PIECES)),
        dma((levels, PIECES)),
        dma((levels, PIECES)),
    ] + [dma((outer - 1,))] * 8 + [dma((tiles,))] * 2 + [dma((outer - 1, 2))] * 2
    return pl.pallas_call(
        functools.partial(kernel, n_sp, n_tp),
        out_shape=jax.ShapeDtypeStruct((chunk, width), BF16),
        in_specs=[hbm] * 7 + [pl.BlockSpec(memory_space=pltpu.SMEM)] + [hbm] * 3,
        out_specs=pl.BlockSpec(memory_space=pltpu.VMEM),
        scratch_shapes=scratch,
        compiler_params=pltpu.CompilerParams(
            collective_id=0, has_side_effects=True, vmem_limit_bytes=67043328
        ),
    )(gate, mix, inp, taps, q, k, v, lam, gain.reshape(1, -1), wc, wh)


def solution(mesh):
    placed = (
        P("sp", "tp"),
        P("sp", "tp"),
        P("sp", "tp"),
        P(None, "tp"),
        P("sp", "tp"),
        P("sp", "tp"),
        P("sp", "tp"),
        P("tp"),
        P(),
        P("tp", None),
        P("tp", None),
    )
    return jax.shard_map(
        functools.partial(shards, mesh.shape["sp"], mesh.shape["tp"]),
        mesh=mesh,
        in_specs=placed,
        out_specs=P(("sp", "tp"), None),
        check_vma=False,
    )
```

profile of v0, /device:TPU:25, one launch (start us, length us, event | category | flops | bytes accessed | tf_op | source)
XLA Modules:
  0.0 26.0 jit_solution(106798621481219246)
XLA Ops:
  0.7 23.7 %shard_map.109 = bf16[64,2048]{1,0:T(8,128)(2,1)} custom-call(bf16[256,128]{1,0:T(8,128)(2,1)} %gate_h.1, bf16[256,128]{1,0:T(8,128)(2,1)} %mix_h.1, bf16[256,128]{1,0:T(8,128)(2,1)} %inp_h.1, bf16[3,128]{1,0:T(4,128)(2,1)} %taps_h.1, bf16[256,128]{1,0:T(8,128)(2,1)} %q_h.1, bf16[256,128]{1,0:T(8,128)(2,1)} %k_h.1, bf16[256,128]{1,0:T(8,128)(2,1)} %v_h.1, ...), custom_call_target="tpu_custom_call" | custom-call | tf_op jit(solution)/shard_map/pallas_call | solution.py:538
  24.4 1.7 %copy.14 = bf16[64,2048]{1,0:T(8,128)(2,1)} copy(bf16[64,2048]{1,0:T(8,128)(2,1)} %shard_map.109) | data formatting | bytes 524288
where the time goes:
time: 26.2 us; the launch traced here: 26 us
  Pallas kernels  23.7 us (90%)
  local copies, waits for them, and re-layouts  1.67 us (6%)
  between operations  0.66 us (3%)
    pallas_call x1, Pallas kernels, shards(): pl.pallas_call(functools.partial(kernel, n_sp, n_tp), out_shape=jax.Shape...  23.7 us
    unnamed x1, local copies, waits for them, and re-layouts  1.67 us

commit v1 on v0

--- a/solution.py
+++ b/solution.py
@@ -537,12 +537,12 @@
     ] + [dma((outer - 1,))] * 8 + [dma((tiles,))] * 2 + [dma((outer - 1, 2))] * 2
     return pl.pallas_call(
         functools.partial(kernel, n_sp, n_tp),
-        out_shape=jax.ShapeDtypeStruct((chunk, width), BF16),
+        out_shape=pltpu.VMEM((chunk, width), BF16),
         in_specs=[hbm] * 7 + [pl.BlockSpec(memory_space=pltpu.SMEM)] + [hbm] * 3,
         out_specs=pl.BlockSpec(memory_space=pltpu.VMEM),
         scratch_shapes=scratch,
         compiler_params=pltpu.CompilerParams(
-            collective_id=0, has_side_effects=True, vmem_limit_bytes=67043328
+            collective_id=0, has_side_effects=True, vmem_limit_bytes=66000000
         ),
     )(gate, mix, inp, taps, q, k, v, lam, gain.reshape(1, -1), wc, wh)
 

time: 26.2 us -> 24.5 us (0.935)
  local copies, waits for them, and re-layouts: 1.67 us -> 0.71 us
  Pallas kernels: 23.7 us -> 23 us
    unnamed x1, local copies, waits for them, and re-layouts: 1.67 us -> 0.71 us
    pallas_call x1, Pallas kernels: 23.7 us -> 23 us  [shards(): pl.pallas_call(functools.partial(kernel, n_sp, n_tp), out_shape=pltpu.VME...]
where the time goes in v1:
time: 24.5 us; the launch traced here: 24.4 us
  Pallas kernels  23 us (94%)
  local copies, waits for them, and re-layouts  0.71 us (3%)
  between operations  0.66 us (3%)
    pallas_call x1, Pallas kernels, shards(): pl.pallas_call(functools.partial(kernel, n_sp, n_tp), out_shape=pltpu.VME...  23 us
    unnamed x1, local copies, waits for them, and re-layouts  0.71 us

profile of v1, /device:TPU:25, one launch (start us, length us, event | category | flops | bytes accessed | tf_op | source)
XLA Modules:
  0.0 24.4 jit_solution(16779910095613069809)
XLA Ops:
  0.7 23.0 %shard_map.109 = bf16[64,2048]{1,0:T(8,128)(2,1)S(1)} custom-call(bf16[256,128]{1,0:T(8,128)(2,1)} %gate_h.1, bf16[256,128]{1,0:T(8,128)(2,1)} %mix_h.1, bf16[256,128]{1,0:T(8,128)(2,1)} %inp_h.1, bf16[3,128]{1,0:T(4,128)(2,1)} %taps_h.1, bf16[256,128]{1,0:T(8,128)(2,1)} %q_h.1, bf16[256,128]{1,0:T(8,128)(2,1)} %k_h.1, bf16[256,128]{1,0:T(8,128)(2,1)} %v_h.1, ...), custom_call_target="tpu_custom_call" | custom-call | tf_op jit(solution)/shard_map/pallas_call | solution.py:538
  23.7 0.7 %copy.13 = bf16[64,2048]{1,0:T(8,128)(2,1)} copy(bf16[64,2048]{1,0:T(8,128)(2,1)S(1)} %shard_map.109) | data formatting | bytes 524288

commit v2 on v1

v2 whole, which is shorter than its diff:
```python
import functools

import jax
import jax.numpy as jnp
from jax import lax
from jax.experimental import pallas as pl
from jax.experimental.pallas import tpu as pltpu
from jax.sharding import PartitionSpec as P

HEAD_QK = 64
PIECES = 4
GROUPS = 4
UPWARD = (3,)
DOWNWARD = (0, 1)
COL_TILE = 512
MESH = pl.DeviceIdType.MESH
F32 = jnp.float32
BF16 = jnp.bfloat16


def kernel(
    n_sp,
    n_tp,
    gate_h,
    mix_h,
    inp_h,
    taps_h,
    q_h,
    k_h,
    v_h,
    lam_ref,
    gain_h,
    wc_h,
    wh_h,
    out_ref,
    gate,
    mix,
    inp,
    taps,
    gain,
    q,
    col,
    cross,
    halo,
    ext,
    conv,
    wc,
    wh,
    cys,
    cyr,
    own,
    head,
    heads,
    peak,
    acc,
    load_sem,
    halo_ss,
    halo_rs,
    up_ss,
    col_rs,
    x_ss,
    cross_rs,
    mate_ss,
    mate_rs,
    cy_ss,
    cy_rs,
    ha_ss,
    ha_rs,
    wy_ss,
    wy_rs,
    wz_ss,
    wz_rs,
    wf_ss,
    wf_rs,
):
    s = lax.axis_index("sp")
    t = lax.axis_index("tp")
    levels, outer = n_sp // 2, n_tp // 2
    z, x = s // 2, s % 2
    a, b = t // 2, t % 2
    mate = a * 2 + 1 - b
    rows, depth = q.shape
    width = out_ref.shape[1]
    chunk = rows // n_tp
    piece = rows // PIECES
    share = depth // GROUPS
    has_next = s < n_sp - 1
    has_prev = s > 0
    has_up = z < levels - 1
    has_down = z > 0
    paired = levels % 2 == 0
    odd = z % 2 == 1
    upward, downward = (UPWARD, DOWNWARD) if paired else ((), ())
    rest = tuple(g for g in range(GROUPS) if g not in upward + downward)
    even_groups, odd_groups = upward + rest, downward + rest

    def at(sp, tp):
        return {"device_id": (sp, tp), "device_id_type": MESH}

    barrier = pltpu.get_barrier_semaphore()
    ups, downs, side = (z + 1) * 2 + x, (z - 1) * 2 + x, z * 2 + 1 - x

    def greet(sp, tp):
        pl.semaphore_signal(barrier, inc=1, **at(sp, tp))

    pl.when(has_next)(lambda: greet(s + 1, t))
    pl.when(has_prev)(lambda: greet(s - 1, t))
    pl.when(has_up)(lambda: greet(ups, t))
    pl.when(has_down)(lambda: greet(downs, t))
    greet(side, t)
    for step in range(1, n_tp):
        greet(s, lax.rem(t + step, n_tp))

    def held(index, size=depth):
        return pl.ds(pl.multiple_of(index * size, size), size)

    kv = [(h.at[pl.ds(p * piece, piece)], col.at[z, i, pl.ds(p * piece, piece)]) for p in range(PIECES) for i, h in enumerate((k_h, v_h))]
    loads = [
        pltpu.make_async_copy(source, target, load_sem.at[index])
        for index, (source, target) in enumerate(
            [(mix_h, mix), (inp_h, inp)]
            + kv
            + [
                (q_h, q),
                (wh_h, wh.at[held(t)]),
                (wc_h, wc.at[held(b)]),
                (gate_h, gate),
                (taps_h, taps),
                (gain_h, gain),
            ]
        )
    ]
    for load in loads:
        load.start()
    ld_mix, ld_inp = loads[:2]
    own_kv = loads[2 : 2 + 2 * PIECES]
    ld_q, ld_wh, ld_wc, ld_gate, ld_taps, ld_gain = loads[2 + 2 * PIECES :]

    pl.semaphore_wait(
        barrier,
        n_tp
        + has_next.astype(jnp.int32)
        + has_prev.astype(jnp.int32)
        + has_up.astype(jnp.int32)
        + has_down.astype(jnp.int32),
    )

    def part(blocks, level, p):
        return blocks.at[level, :, pl.ds(p * piece, piece), :]

    def up_copy(level, p):
        return pltpu.make_async_remote_copy(
            part(col, level, p), part(col, level, p), up_ss.at[level, p], col_rs.at[level, p], **at(ups, t)
        )

    def x_copy(level, p):
        return pltpu.make_async_remote_copy(
            part(col, level, p), part(cross, level, p), x_ss.at[level, p], cross_rs.at[level, p], **at(side, t)
        )

    def halo_copy(source, slot):
        return pltpu.make_async_remote_copy(
            source.at[pl.ds(rows - 16, 16)], halo.at[slot], halo_ss.at[slot], halo_rs.at[slot], **at(s + 1, t)
        )

    def mate_copy(source, target, slot):
        return pltpu.make_async_remote_copy(source, target, mate_ss.at[slot], mate_rs.at[slot], **at(s, mate))

    def forward(level, p, across=True):
        pl.when(has_up)(lambda: up_copy(level, p).start())
        if across is True:
            x_copy(level, p).start()
        else:
            pl.when(across)(lambda: x_copy(level, p).start())

    ld_mix.wait()
    ld_inp.wait()

    @pl.when(has_next)
    def _():
        halo_copy(mix, 0).start()
        halo_copy(inp, 1).start()

    for p in range(PIECES):
        own_kv[2 * p].wait()
        own_kv[2 * p + 1].wait()
        forward(z, p, x == 0)

    steps = range(1, outer)

    def sent(g):
        return wh.at[held(t * GROUPS + g, share)]

    def theirs(step, g):
        source = lax.rem(a - step + outer, outer) * 2 + b
        return wh.at[held(source * GROUPS + g, share)]

    def wy_copy(step, g):
        other = lax.rem(a + step, outer)
        return pltpu.make_async_remote_copy(
            sent(g), sent(g), wy_ss.at[step - 1, g], wy_rs.at[step - 1, g], **at(s, other * 2 + b)
        )

    def wz_copy(step, g, target):
        ref = theirs(step, g)
        return pltpu.make_async_remote_copy(
            ref, ref, wz_ss.at[step - 1, g], wz_rs.at[step - 1, g], **at(target, t)
        )

    def wf_copy(step, g):
        ref = theirs(step, g)
        return pltpu.make_async_remote_copy(
            ref, ref, wf_ss.at[step - 1, g], wf_rs.at[step - 1, g], **at(s, mate)
        )

    def by_parity(on_odd, on_even):
        pl.when(odd)(on_odd)
        pl.when(jnp.logical_not(odd))(on_even)

    def send_groups(groups):
        def send():
            for g in groups:
                for step in steps:
                    wy_copy(step, g).start()

        return send

    wh_copy = mate_copy(wh.at[held(t)], wh.at[held(t)], 0)
    wc_copy = mate_copy(wc.at[held(b)], wc.at[held(b)], 1)
    lanes = pl.ds(pl.multiple_of(b * depth, depth), depth)
    conv_copy = mate_copy(conv.at[:, lanes], conv.at[:, lanes], 2)

    ld_wh.wait()
    by_parity(send_groups(odd_groups), send_groups(even_groups))
    ld_wc.wait()
    wc_copy.start()
    wh_copy.start()

    ld_q.wait()
    scale = HEAD_QK ** (-0.5)
    q[...] = (q[...].astype(F32) * scale).astype(BF16)

    def scores_of(block, m):
        pair = slice(m * HEAD_QK, (m + 1) * HEAD_QK)
        return lax.dot_general(
            q[:, pair], block[0, :, pair], (((1,), (1,)), ((), ())), preferred_element_type=F32
        )

    ones = jnp.ones((rows, depth), BF16)

    def spread(top, lanes_of):
        return jnp.concatenate([top] * (lanes_of // depth), axis=1) if lanes_of > depth else top

    def attend(blocks, first=False):
        scored = [[scores_of(block, m) for block in blocks] for m in range(2)]
        if first:
            ahead = lax.broadcasted_iota(jnp.int32, (rows, rows), 0)
            keys = lax.broadcasted_iota(jnp.int32, (rows, rows), 1)
            scored = [[jnp.where(keys <= ahead, scores, -jnp.inf) for scores in of] for of in scored]
        tops = [jnp.max(functools.reduce(jnp.maximum, of), axis=1, keepdims=True) for of in scored]
        for m in range(2):
            top = jnp.broadcast_to(tops[m], (rows, depth))
            if not first:
                before = peak[m]
                top = jnp.maximum(before, top)
                total = acc[m] * spread(jnp.exp(before - top), 2 * depth)
            wide = spread(top, rows)
            for index, (scores, block) in enumerate(zip(scored[m], blocks)):
                weights = jnp.exp(scores - wide).astype(BF16)
                add = jnp.dot(weights, jnp.concatenate([block[1], ones], axis=1), preferred_element_type=F32)
                total = add if first and index == 0 else total + add
            peak[m] = top
            acc[m] = total

    attend([col.at[z]], True)

    def gated(u, v):
        return (u.astype(F32) * v.astype(F32)).astype(BF16).astype(F32)

    def rows_of(oa, ob):
        return pl.ds(pl.multiple_of((oa * 2 + ob) * chunk, chunk), chunk)

    tiles = [slice(c, c + COL_TILE) for c in range(0, width, COL_TILE)]

    def cy_copy(step):
        other = lax.rem(a + step, outer)
        return pltpu.make_async_remote_copy(
            cys.at[step - 1], cyr.at[step - 1], cy_ss.at[step - 1], cy_rs.at[step - 1], **at(s, other * 2 + b)
        )

    def convolve():
        ext[pl.ds(8, rows), :] = gated(mix[...], inp[...])

        @pl.when(has_prev)
        def _():
            halo_copy(mix, 0).wait_recv()
            halo_copy(inp, 1).wait_recv()
            ext[pl.ds(0, 8), :] = gated(halo[0], halo[1])[8:16]

        @pl.when(jnp.logical_not(has_prev))
        def _():
            ext[pl.ds(0, 8), :] = jnp.zeros((8, ext.shape[1]), F32)

        ld_gate.wait()
        ld_taps.wait()
        taps_v = taps[...].astype(F32)
        conv[:, lanes] = (
            gate[...].astype(F32)
            * (
                taps_v[0:1] * ext[pl.ds(6, rows), :]
                + taps_v[1:2] * ext[pl.ds(7, rows), :]
                + taps_v[2:3] * ext[pl.ds(8, rows), :]
            )
        ).astype(BF16)
        conv_copy.start()

    def project_conv():
        wc_copy.wait_recv()
        conv_copy.wait_recv()
        for step in steps:
            other = lax.rem(a + step, outer)
            for tile in tiles:
                cys[step - 1, :, tile] = jnp.dot(
                    conv[rows_of(other, b), :], wc[:, tile], preferred_element_type=F32
                ).astype(BF16)
            cy_copy(step).start()
        for tile in tiles:
            own[:, tile] = jnp.dot(conv[rows_of(a, b), :], wc[:, tile], preferred_element_type=F32)

    def take(groups, target=None):
        for g in groups:
            for step in steps:
                wy_copy(step, g).wait_recv()
                if target is not None:
                    wz_copy(step, g, target).start()
                wf_copy(step, g).start()

    def take_from(groups, target):
        for g in groups:
            for step in steps:
                wz_copy(step, g, target).wait_recv()
                wf_copy(step, g).start()

    def stage_a():
        by_parity(lambda: take(downward[:1], downs), lambda: take(upward, ups))

    def stage_b():
        by_parity(lambda: take(downward[1:], downs), lambda: take(rest))

    def stage_c():
        by_parity(lambda: take(rest), lambda: take_from(downward, ups))

    def stage_d():
        pl.when(odd)(lambda: take_from(upward, downs))

    def convolve_s():
        convolve()

    def project_s():
        project_conv()

    @pl.when(z == 0)
    def _():
        convolve_s()
        project_s()

    def pieces(level, low, high):
        for p in range(low, high):
            up_copy(level, p).wait_recv()
            forward(level, p)

    def await_cross(level):
        for p in range(PIECES):
            x_copy(level, p).wait_recv()

    def attend_pair(level, crossed, both):
        @pl.when(both)
        def _():
            await_cross(crossed)
            attend([cross.at[crossed], col.at[level]])

        @pl.when(jnp.logical_not(both))
        def _():
            attend([col.at[level]])

    def advance(k, carry):
        level = z - k
        pieces(level, 0, PIECES // 2)
        pl.when(k > 1)(lambda: attend_pair(level + 1, jnp.minimum(level + 2, z), jnp.logical_or(k > 2, x == 1)))
        pl.when(k == 3)(stage_b)
        pieces(level, PIECES // 2, PIECES)
        pl.when(k == 1)(convolve_s)

        @pl.when(k == 2)
        def _():
            project_s()
            stage_a()

        return carry

    lax.fori_loop(1, z + 1, advance, 0)
    pl.when(z > 0)(lambda: attend_pair(0, jnp.minimum(1, z), jnp.logical_or(z > 1, x == 1)))

    @pl.when(z == 1)
    def _():
        project_s()
        stage_a()

    pl.when(jnp.logical_and(z > 0, z < 3))(stage_b)
    soon = jnp.logical_and(z > 2, odd)
    pl.when(soon)(stage_c)

    @pl.when(jnp.logical_or(z > 0, x == 1))
    def _():
        await_cross(0)
        attend([cross.at[0]])

    ld_gain.wait()

    def merge(oa):
        chosen = pl.ds(pl.multiple_of(oa * 2 * chunk, 2 * chunk), 2 * chunk)
        merged = acc[0, chosen, :depth] / acc[0, chosen, depth:] - lam_ref[0] * (
            acc[1, chosen, :depth] / acc[1, chosen, depth:]
        )
        norm = lax.rsqrt(jnp.mean(merged * merged, axis=1, keepdims=True) + 1e-06)
        head[chosen, :] = (merged * norm * gain[...] * 0.8).astype(BF16)

    mine = pl.ds(pl.multiple_of(t * depth, depth), depth)

    def ha_copy(step, ob):
        other = lax.rem(a + step, outer)
        return pltpu.make_async_remote_copy(
            head.at[rows_of(other, ob)],
            heads.at[:, mine],
            ha_ss.at[step - 1, ob],
            ha_rs.at[step - 1, b],
            **at(s, other * 2 + ob),
        )

    def ha_arrival(step, ob):
        return pltpu.make_async_remote_copy(
            head.at[rows_of(a, b)],
            heads.at[:, mine],
            ha_ss.at[step - 1, ob],
            ha_rs.at[step - 1, ob],
            **at(s, mate),
        )

    mate_head = mate_copy(head.at[rows_of(a, 1 - b)], heads.at[:, mine], 3)
    for step in steps:
        merge(lax.rem(a + step, outer))
        for ob in range(2):
            ha_copy(step, ob).start()
    merge(a)
    mate_head.start()
    heads[:, mine] = head[rows_of(a, b), :]

    @pl.when(z == 0)
    def _():
        stage_a()
        stage_b()

    pl.when(jnp.logical_not(soon))(stage_c)
    stage_d()

    def product(oa, tile):
        k = held(oa, 2 * depth)
        return jnp.dot(heads[:, k], wh[k, tile], preferred_element_type=F32)

    wh_copy.wait_recv()
    mate_head.wait_recv()
    for tile in tiles:
        own[:, tile] += product(a, tile)
    for step in steps:
        cy_copy(step).wait_recv()
    for step in steps:
        for g in range(GROUPS):
            wf_copy(step, g).wait_recv()
    for step in steps:
        for ob in range(2):
            ha_arrival(step, ob).wait_recv()
    for tile in tiles:
        total = own[:, tile]
        for step in steps:
            total = total + cyr[step - 1, :, tile].astype(F32) + product(lax.rem(a + step, outer), tile)
        out_ref[:, tile] = total.astype(out_ref.dtype)


    def drain(level, carry):
        for p in range(PIECES):
            pl.when(has_up)(lambda: up_copy(level, p).wait_send())
            pl.when(jnp.logical_or(level < z, x == 0))(lambda: x_copy(level, p).wait_send())
        return carry

    lax.fori_loop(0, z + 1, drain, 0)

    @pl.when(has_next)
    def _():
        halo_copy(mix, 0).wait_send()
        halo_copy(inp, 1).wait_send()

    def drain_groups(sent_groups, passed, target):
        def run():
            for step in steps:
                for g in sent_groups:
                    wy_copy(step, g).wait_send()
                for g in passed:
                    wz_copy(step, g, target).wait_send()

        return run

    by_parity(drain_groups(odd_groups, downward, downs), drain_groups(even_groups, upward, ups))
    for copy in (wh_copy, wc_copy, conv_copy, mate_head):
        copy.wait_send()
    for step in steps:
        for g in range(GROUPS):
            wf_copy(step, g).wait_send()
        cy_copy(step).wait_send()
        for ob in range(2):
            ha_copy(step, ob).wait_send()


def shards(n_sp, n_tp, *args):
    gate, mix, inp, taps, q, k, v, lam, gain, wc, wh = args
    rows, lanes = q.shape
    depth, width = wh.shape
    levels, outer = n_sp // 2, n_tp // 2
    chunk = rows // n_tp
    dma = pltpu.SemaphoreType.DMA
    hbm = pl.BlockSpec(memory_space=pltpu.HBM)
    scratch = [
        pltpu.VMEM(gate.shape, BF16),
        pltpu.VMEM(mix.shape, BF16),
        pltpu.VMEM(inp.shape, BF16),
        pltpu.VMEM(taps.shape, BF16),
        pltpu.VMEM((1, gain.shape[0]), F32),
        pltpu.VMEM(q.shape, BF16),
        pltpu.VMEM((levels, 2, rows, lanes), BF16),
        pltpu.VMEM((levels, 2, rows, lanes), BF16),
        pltpu.VMEM((2, 16, mix.shape[1]), BF16),
        pltpu.VMEM((rows + 8, mix.shape[1]), F32),
        pltpu.VMEM((rows, 2 * lanes), BF16),
        pltpu.VMEM((2 * depth, width), BF16),
        pltpu.VMEM((n_tp * depth, width), BF16),
        pltpu.VMEM((outer - 1, chunk, width), BF16),
        pltpu.VMEM((outer - 1, chunk, width), BF16),
        pltpu.VMEM((chunk, width), F32),
        pltpu.VMEM((rows, depth), BF16),
        pltpu.VMEM((chunk, n_tp * depth), BF16),
        pltpu.VMEM((2, rows, depth), F32),
        pltpu.VMEM((2, rows, 2 * depth), F32),
        dma((2 * PIECES + 8,)),
        dma((2,)),
        dma((2,)),
        dma((levels, PIECES)),
        dma((levels, PIECES)),
        dma((levels, PIECES)),
        dma((levels, PIECES)),
        dma((4,)),
        dma((4,)),
        dma((outer - 1,)),
        dma((outer - 1,)),
        dma((outer - 1, 2)),
        dma((outer - 1, 2)),
    ] + [dma((outer - 1, GROUPS))] * 6
    return pl.pallas_call(
        functools.partial(kernel, n_sp, n_tp),
        out_shape=pltpu.VMEM((chunk, width), BF16),
        in_specs=[hbm] * 7 + [pl.BlockSpec(memory_space=pltpu.SMEM)] + [hbm] * 3,
        out_specs=pl.BlockSpec(memory_space=pltpu.VMEM),
        scratch_shapes=scratch,
        compiler_params=pltpu.CompilerParams(
            collective_id=0, has_side_effects=True, vmem_limit_bytes=66000000
        ),
    )(gate, mix, inp, taps, q, k, v, lam, gain.reshape(1, -1), wc, wh)


def solution(mesh):
    placed = (
        P("sp", "tp"),
        P("sp", "tp"),
        P("sp", "tp"),
        P(None, "tp"),
        P("sp", "tp"),
        P("sp", "tp"),
        P("sp", "tp"),
        P("tp"),
        P(),
        P("tp", None),
        P("tp", None),
    )
    return jax.shard_map(
        functools.partial(shards, mesh.shape["sp"], mesh.shape["tp"]),
        mesh=mesh,
        in_specs=placed,
        out_specs=P(("sp", "tp"), None),
        check_vma=False,
    )
```

time: 24.5 us -> 22.8 us (0.931)
  Pallas kernels: 23 us -> 21.3 us
    pallas_call x1, Pallas kernels: 23 us -> 21.3 us  [shards(): pl.pallas_call(functools.partial(kernel, n_sp, n_tp), out_shape=pltpu.VME...]
where the time goes in v2:
time: 22.8 us; the launch traced here: 22.6 us
  Pallas kernels  21.3 us (93%)
  local copies, waits for them, and re-layouts  0.71 us (3%)
  between operations  0.66 us (3%)
    pallas_call x1, Pallas kernels, shards(): pl.pallas_call(functools.partial(kernel, n_sp, n_tp), out_shape=pltpu.VME...  21.3 us
    unnamed x1, local copies, waits for them, and re-layouts  0.71 us

profile of v2, /device:TPU:25, one launch (start us, length us, event | category | flops | bytes accessed | tf_op | source)
XLA Modules:
  0.0 22.6 jit_solution(8495413535863598717)
XLA Ops:
  0.7 21.3 %shard_map.109 = bf16[64,2048]{1,0:T(8,128)(2,1)S(1)} custom-call(bf16[256,128]{1,0:T(8,128)(2,1)} %gate_h.1, bf16[256,128]{1,0:T(8,128)(2,1)} %mix_h.1, bf16[256,128]{1,0:T(8,128)(2,1)} %inp_h.1, bf16[3,128]{1,0:T(4,128)(2,1)} %taps_h.1, bf16[256,128]{1,0:T(8,128)(2,1)} %q_h.1, bf16[256,128]{1,0:T(8,128)(2,1)} %k_h.1, bf16[256,128]{1,0:T(8,128)(2,1)} %v_h.1, ...), custom_call_target="tpu_custom_call" | custom-call | tf_op jit(solution)/shard_map/pallas_call | solution.py:566
  21.9 0.7 %copy.13 = bf16[64,2048]{1,0:T(8,128)(2,1)} copy(bf16[64,2048]{1,0:T(8,128)(2,1)S(1)} %shard_map.109) | data formatting | bytes 524288

commit v3 on v2

--- a/solution.py
+++ b/solution.py
@@ -33,15 +33,14 @@
     wc_h,
     wh_h,
     out_ref,
-    gate,
-    mix,
-    inp,
+    mi,
+    qg,
     taps,
     gain,
-    q,
     col,
     cross,
     halo,
+    relay,
     ext,
     conv,
     wc,
@@ -60,6 +59,9 @@
     col_rs,
     x_ss,
     cross_rs,
+    ex_ss,
+    eu_ss,
+    e_rs,
     mate_ss,
     mate_rs,
     cy_ss,
@@ -79,12 +81,13 @@
     z, x = s // 2, s % 2
     a, b = t // 2, t % 2
     mate = a * 2 + 1 - b
-    rows, depth = q.shape
+    _, rows, depth = qg.shape
+    mix, inp, q, gate = mi.at[0], mi.at[1], qg.at[0], qg.at[1]
+    half = rows // 2
     width = out_ref.shape[1]
     chunk = rows // n_tp
     piece = rows // PIECES
     share = depth // GROUPS
-    has_next = s < n_sp - 1
     has_prev = s > 0
     has_up = z < levels - 1
     has_down = z > 0
@@ -103,8 +106,6 @@
     def greet(sp, tp):
         pl.semaphore_signal(barrier, inc=1, **at(sp, tp))
 
-    pl.when(has_next)(lambda: greet(s + 1, t))
-    pl.when(has_prev)(lambda: greet(s - 1, t))
     pl.when(has_up)(lambda: greet(ups, t))
     pl.when(has_down)(lambda: greet(downs, t))
     greet(side, t)
@@ -114,104 +115,147 @@
     def held(index, size=depth):
         return pl.ds(pl.multiple_of(index * size, size), size)
 
-    kv = [(h.at[pl.ds(p * piece, piece)], col.at[z, i, pl.ds(p * piece, piece)]) for p in range(PIECES) for i, h in enumerate((k_h, v_h))]
     loads = [
         pltpu.make_async_copy(source, target, load_sem.at[index])
-        for index, (source, target) in enumerate(
-            [(mix_h, mix), (inp_h, inp)]
-            + kv
-            + [
-                (q_h, q),
-                (wh_h, wh.at[held(t)]),
-                (wc_h, wc.at[held(b)]),
-                (gate_h, gate),
-                (taps_h, taps),
-                (gain_h, gain),
-            ]
+        for source, target, index in (
+            (k_h, col.at[z, 0], 0),
+            (v_h, col.at[z, 1], 0),
+            (mix_h, mix, 1),
+            (inp_h, inp, 1),
+            (q_h, q, 2),
+            (gate_h, gate, 2),
+            (wh_h, wh.at[held(t)], 3),
+            (wc_h, wc.at[held(b)], 4),
+            (taps_h, taps, 5),
+            (gain_h, gain, 6),
         )
     ]
     for load in loads:
         load.start()
-    ld_mix, ld_inp = loads[:2]
-    own_kv = loads[2 : 2 + 2 * PIECES]
-    ld_q, ld_wh, ld_wc, ld_gate, ld_taps, ld_gain = loads[2 + 2 * PIECES :]
-
-    pl.semaphore_wait(
-        barrier,
-        n_tp
-        + has_next.astype(jnp.int32)
-        + has_prev.astype(jnp.int32)
-        + has_up.astype(jnp.int32)
-        + has_down.astype(jnp.int32),
-    )
+    ld_wh, ld_wc, ld_taps, ld_gain = loads[6:]
+
+    def loaded(both, index):
+        return pltpu.make_async_copy(both, both, load_sem.at[index])
+
+    pl.semaphore_wait(barrier, n_tp + has_up.astype(jnp.int32) + has_down.astype(jnp.int32))
 
     def part(blocks, level, p):
         return blocks.at[level, :, pl.ds(p * piece, piece), :]
 
     def up_copy(level, p):
         return pltpu.make_async_remote_copy(
-            part(col, level, p), part(col, level, p), up_ss.at[level, p], col_rs.at[level, p], **at(ups, t)
+            part(col, level, p), part(col, level, p), up_ss.at[level], col_rs.at[level, p], **at(ups, t)
+        )
+
+    def up_all(level):
+        return pltpu.make_async_remote_copy(
+            col.at[level], col.at[level], up_ss.at[level], col_rs.at[level, 0], **at(ups, t)
         )
 
     def x_copy(level, p):
         return pltpu.make_async_remote_copy(
-            part(col, level, p), part(cross, level, p), x_ss.at[level, p], cross_rs.at[level, p], **at(side, t)
-        )
-
-    def halo_copy(source, slot):
-        return pltpu.make_async_remote_copy(
-            source.at[pl.ds(rows - 16, 16)], halo.at[slot], halo_ss.at[slot], halo_rs.at[slot], **at(s + 1, t)
-        )
+            part(col, level, p), part(cross, level, p), x_ss.at[level], cross_rs.at[level], **at(side, t)
+        )
+
+    def x_all(level):
+        return pltpu.make_async_remote_copy(
+            col.at[level], cross.at[level], x_ss.at[level], cross_rs.at[level], **at(side, t)
+        )
+
+    first_half = pl.ds(0, half)
+
+    def x_half(level):
+        return pltpu.make_async_remote_copy(
+            col.at[level, :, first_half, :], cross.at[level, :, first_half, :], x_ss.at[level], cross_rs.at[level], **at(side, t)
+        )
+
+    early, extra = range(PIECES // 2), range(PIECES // 2, PIECES)
+
+    def ex_copy(p):
+        return pltpu.make_async_remote_copy(
+            part(col, 0, p), part(cross, 0, p), ex_ss.at[0], e_rs.at[p - PIECES // 2], **at(side, t)
+        )
+
+    def eu_copy(p):
+        ref = part(cross, 0, p)
+        return pltpu.make_async_remote_copy(ref, ref, eu_ss.at[0], e_rs.at[p - PIECES // 2], **at(ups, t))
+
+    def half_sent(sem):
+        ref = cross.at[0, :, first_half, :]
+        return pltpu.make_async_remote_copy(ref, ref, sem.at[0], e_rs.at[0], **at(side, t))
+
+    edge = mi.at[:, pl.ds(rows - 16, 16), :]
+
+    def halo_copy(source, target, slot, to):
+        return pltpu.make_async_remote_copy(source, target, halo_ss.at[slot], halo_rs.at[slot], **at(to, t))
+
+    halo_side = halo_copy(edge, halo, 0, side)
+    halo_up = halo_copy(edge, relay, 1, ups)
+    halo_pass = halo_copy(relay, halo, 0, side)
 
     def mate_copy(source, target, slot):
-        return pltpu.make_async_remote_copy(source, target, mate_ss.at[slot], mate_rs.at[slot], **at(s, mate))
-
-    def forward(level, p, across=True):
+        return pltpu.make_async_remote_copy(source, target, mate_ss.at[max(slot - 1, 0)], mate_rs.at[slot], **at(s, mate))
+
+    def forward(level, p):
         pl.when(has_up)(lambda: up_copy(level, p).start())
-        if across is True:
+        if p in early:
             x_copy(level, p).start()
         else:
-            pl.when(across)(lambda: x_copy(level, p).start())
-
-    ld_mix.wait()
-    ld_inp.wait()
-
-    @pl.when(has_next)
-    def _():
-        halo_copy(mix, 0).start()
-        halo_copy(inp, 1).start()
-
-    for p in range(PIECES):
-        own_kv[2 * p].wait()
-        own_kv[2 * p + 1].wait()
-        forward(z, p, x == 0)
+            pl.when(level > 0)(lambda: x_copy(level, p).start())
+
+    loaded(mi, 1).wait()
+    pl.when(x == 0)(lambda: halo_side.start())
+    pl.when(jnp.logical_and(x == 1, has_up))(lambda: halo_up.start())
+    loaded(col.at[z], 0).wait()
+
+    @pl.when(has_up)
+    def _():
+        for p in range(PIECES):
+            up_copy(z, p).start()
+
+    @pl.when(z == 0)
+    def _():
+        for p in extra:
+            ex_copy(p).start()
+
+    @pl.when(x == 0)
+    def _():
+        for p in early:
+            x_copy(z, p).start()
+
+        @pl.when(z > 0)
+        def _():
+            for p in extra:
+                x_copy(z, p).start()
 
     steps = range(1, outer)
 
     def sent(g):
         return wh.at[held(t * GROUPS + g, share)]
 
-    def theirs(step, g):
-        source = lax.rem(a - step + outer, outer) * 2 + b
-        return wh.at[held(source * GROUPS + g, share)]
-
-    def wy_copy(step, g):
+    def wy_copy(step, g, place):
         other = lax.rem(a + step, outer)
         return pltpu.make_async_remote_copy(
-            sent(g), sent(g), wy_ss.at[step - 1, g], wy_rs.at[step - 1, g], **at(s, other * 2 + b)
-        )
-
-    def wz_copy(step, g, target):
-        ref = theirs(step, g)
-        return pltpu.make_async_remote_copy(
-            ref, ref, wz_ss.at[step - 1, g], wz_rs.at[step - 1, g], **at(target, t)
-        )
-
-    def wf_copy(step, g):
-        ref = theirs(step, g)
-        return pltpu.make_async_remote_copy(
-            ref, ref, wf_ss.at[step - 1, g], wf_rs.at[step - 1, g], **at(s, mate)
-        )
+            sent(g), sent(g), wy_ss.at[step - 1], wy_rs.at[step - 1, place], **at(s, other * 2 + b)
+        )
+
+    def region(index, groups):
+        return wh.at[pl.ds(pl.multiple_of(index * depth + groups[0] * share, share), len(groups) * share)]
+
+    def source_of(step):
+        return lax.rem(a - step + outer, outer) * 2 + b
+
+    def wy_sent(step, groups):
+        ref = region(t, sorted(groups))
+        return pltpu.make_async_remote_copy(ref, ref, wy_ss.at[step - 1], wy_rs.at[step - 1, 0], **at(s, mate))
+
+    def wz_copy(step, groups, target):
+        ref = region(source_of(step), groups)
+        return pltpu.make_async_remote_copy(ref, ref, wz_ss.at[step - 1], wz_rs.at[step - 1], **at(target, t))
+
+    def wf_copy(step, groups):
+        ref = region(source_of(step), groups)
+        return pltpu.make_async_remote_copy(ref, ref, wf_ss.at[step - 1], wf_rs.at[step - 1], **at(s, mate))
 
     def by_parity(on_odd, on_even):
         pl.when(odd)(on_odd)
@@ -219,9 +263,9 @@
 
     def send_groups(groups):
         def send():
-            for g in groups:
+            for place, g in enumerate(groups):
                 for step in steps:
-                    wy_copy(step, g).start()
+                    wy_copy(step, g, place).start()
 
         return send
 
@@ -236,7 +280,12 @@
     wc_copy.start()
     wh_copy.start()
 
-    ld_q.wait()
+    @pl.when(jnp.logical_and(x == 1, z > 0))
+    def _():
+        halo_up.wait_recv()
+        halo_pass.start()
+
+    loaded(qg, 2).wait()
     scale = HEAD_QK ** (-0.5)
     q[...] = (q[...].astype(F32) * scale).astype(BF16)
 
@@ -293,15 +342,13 @@
 
         @pl.when(has_prev)
         def _():
-            halo_copy(mix, 0).wait_recv()
-            halo_copy(inp, 1).wait_recv()
+            halo_side.wait_recv()
             ext[pl.ds(0, 8), :] = gated(halo[0], halo[1])[8:16]
 
         @pl.when(jnp.logical_not(has_prev))
         def _():
             ext[pl.ds(0, 8), :] = jnp.zeros((8, ext.shape[1]), F32)
 
-        ld_gate.wait()
         ld_taps.wait()
         taps_v = taps[...].astype(F32)
         conv[:, lanes] = (
@@ -327,31 +374,44 @@
         for tile in tiles:
             own[:, tile] = jnp.dot(conv[rows_of(a, b), :], wc[:, tile], preferred_element_type=F32)
 
-    def take(groups, target=None):
+    def take(groups, order, passed=None):
         for g in groups:
             for step in steps:
-                wy_copy(step, g).wait_recv()
-                if target is not None:
-                    wz_copy(step, g, target).start()
-                wf_copy(step, g).start()
+                wy_copy(step, g, order.index(g)).wait_recv()
+                if passed is not None:
+                    wz_copy(step, (g,), passed).start()
+                wf_copy(step, (g,)).start()
 
     def take_from(groups, target):
-        for g in groups:
-            for step in steps:
-                wz_copy(step, g, target).wait_recv()
-                wf_copy(step, g).start()
-
-    def stage_a():
-        by_parity(lambda: take(downward[:1], downs), lambda: take(upward, ups))
-
-    def stage_b():
-        by_parity(lambda: take(downward[1:], downs), lambda: take(rest))
-
-    def stage_c():
-        by_parity(lambda: take(rest), lambda: take_from(downward, ups))
-
-    def stage_d():
-        pl.when(odd)(lambda: take_from(upward, downs))
+        for step in steps if groups else ():
+            wz_copy(step, groups, target).wait_recv()
+            wf_copy(step, groups).start()
+
+    def odd_a():
+        take(downward[:1], odd_groups, downs)
+
+    def odd_b():
+        take(downward[1:], odd_groups, downs)
+
+    def odd_c():
+        take(rest, odd_groups)
+
+    def odd_d():
+        take_from(upward, downs)
+
+    def even_a():
+        take(upward, even_groups, ups)
+
+    def even_b():
+        take(rest, even_groups)
+
+    def even_c():
+        take_from(downward, ups)
+
+    def extras():
+        for p in extra:
+            eu_copy(p).wait_recv()
+            pl.when(has_up)(lambda: eu_copy(p).start())
 
     def convolve_s():
         convolve()
@@ -361,6 +421,7 @@
 
     @pl.when(z == 0)
     def _():
+        extras()
         convolve_s()
         project_s()
 
@@ -370,8 +431,7 @@
             forward(level, p)
 
     def await_cross(level):
-        for p in range(PIECES):
-            x_copy(level, p).wait_recv()
+        x_all(level).wait_recv()
 
     def attend_pair(level, crossed, both):
         @pl.when(both)
@@ -386,33 +446,39 @@
     def advance(k, carry):
         level = z - k
         pieces(level, 0, PIECES // 2)
+        pl.when(jnp.logical_and(k == 3, odd))(odd_b)
         pl.when(k > 1)(lambda: attend_pair(level + 1, jnp.minimum(level + 2, z), jnp.logical_or(k > 2, x == 1)))
-        pl.when(k == 3)(stage_b)
+        pl.when(jnp.logical_and(k == 2, odd))(odd_a)
         pieces(level, PIECES // 2, PIECES)
         pl.when(k == 1)(convolve_s)
-
-        @pl.when(k == 2)
-        def _():
-            project_s()
-            stage_a()
+        pl.when(k == 2)(project_s)
 
         return carry
 
     lax.fori_loop(1, z + 1, advance, 0)
-    pl.when(z > 0)(lambda: attend_pair(0, jnp.minimum(1, z), jnp.logical_or(z > 1, x == 1)))
+
+    @pl.when(z > 0)
+    def _():
+        attend_pair(0, jnp.minimum(1, z), jnp.logical_or(z > 1, x == 1))
+        pl.when(z == 1)(odd_a)
+        extras()
 
     @pl.when(z == 1)
     def _():
         project_s()
-        stage_a()
-
-    pl.when(jnp.logical_and(z > 0, z < 3))(stage_b)
+        odd_b()
+
+    @pl.when(jnp.logical_and(z > 1, jnp.logical_not(odd)))
+    def _():
+        even_a()
+        even_b()
+
     soon = jnp.logical_and(z > 2, odd)
-    pl.when(soon)(stage_c)
+    pl.when(soon)(odd_c)
 
     @pl.when(jnp.logical_or(z > 0, x == 1))
     def _():
-        await_cross(0)
+        x_half(0).wait_recv()
         attend([cross.at[0]])
 
     ld_gain.wait()
@@ -432,19 +498,18 @@
         return pltpu.make_async_remote_copy(
             head.at[rows_of(other, ob)],
             heads.at[:, mine],
-            ha_ss.at[step - 1, ob],
-            ha_rs.at[step - 1, b],
+            ha_ss.at[step - 1],
+            ha_rs.at[step - 1],
             **at(s, other * 2 + ob),
         )
 
-    def ha_arrival(step, ob):
-        return pltpu.make_async_remote_copy(
-            head.at[rows_of(a, b)],
-            heads.at[:, mine],
-            ha_ss.at[step - 1, ob],
-            ha_rs.at[step - 1, ob],
-            **at(s, mate),
-        )
+    def ha_sent(step):
+        ref = head.at[pl.ds(pl.multiple_of(lax.rem(a + step, outer) * 2 * chunk, 2 * chunk), 2 * chunk)]
+        return pltpu.make_async_remote_copy(ref, ref, ha_ss.at[step - 1], ha_rs.at[step - 1], **at(s, mate))
+
+    def ha_arrival(step):
+        ref = heads.at[:, held(lax.rem(a - step + outer, outer), 2 * depth)]
+        return pltpu.make_async_remote_copy(ref, ref, ha_ss.at[step - 1], ha_rs.at[step - 1], **at(s, mate))
 
     mate_head = mate_copy(head.at[rows_of(a, 1 - b)], heads.at[:, mine], 3)
     for step in steps:
@@ -457,11 +522,14 @@
 
     @pl.when(z == 0)
     def _():
-        stage_a()
-        stage_b()
-
-    pl.when(jnp.logical_not(soon))(stage_c)
-    stage_d()
+        even_a()
+        even_b()
+
+    def odd_end():
+        pl.when(z < 3)(odd_c)
+        odd_d()
+
+    by_parity(odd_end, even_c)
 
     def product(oa, tile):
         k = held(oa, 2 * depth)
@@ -474,11 +542,9 @@
     for step in steps:
         cy_copy(step).wait_recv()
     for step in steps:
-        for g in range(GROUPS):
-            wf_copy(step, g).wait_recv()
+        wf_copy(step, tuple(range(GROUPS))).wait_recv()
     for step in steps:
-        for ob in range(2):
-            ha_arrival(step, ob).wait_recv()
+        ha_arrival(step).wait_recv()
     for tile in tiles:
         total = own[:, tile]
         for step in steps:
@@ -487,37 +553,35 @@
 
 
     def drain(level, carry):
-        for p in range(PIECES):
-            pl.when(has_up)(lambda: up_copy(level, p).wait_send())
-            pl.when(jnp.logical_or(level < z, x == 0))(lambda: x_copy(level, p).wait_send())
+        pl.when(has_up)(lambda: up_all(level).wait_send())
+        pl.when(jnp.logical_and(level > 0, jnp.logical_or(level < z, x == 0)))(lambda: x_all(level).wait_send())
         return carry
 
     lax.fori_loop(0, z + 1, drain, 0)
-
-    @pl.when(has_next)
-    def _():
-        halo_copy(mix, 0).wait_send()
-        halo_copy(inp, 1).wait_send()
+    pl.when(jnp.logical_or(z > 0, x == 0))(lambda: x_half(0).wait_send())
+    pl.when(z == 0)(lambda: half_sent(ex_ss).wait_send())
+    pl.when(has_up)(lambda: half_sent(eu_ss).wait_send())
+    pl.when(x == 0)(lambda: halo_side.wait_send())
+    pl.when(jnp.logical_and(x == 1, has_up))(lambda: halo_up.wait_send())
+    pl.when(jnp.logical_and(x == 1, z > 0))(lambda: halo_pass.wait_send())
 
     def drain_groups(sent_groups, passed, target):
         def run():
             for step in steps:
-                for g in sent_groups:
-                    wy_copy(step, g).wait_send()
-                for g in passed:
-                    wz_copy(step, g, target).wait_send()
+                wy_sent(step, sent_groups).wait_send()
+                if passed:
+                    wz_copy(step, passed, target).wait_send()
 
         return run
 
     by_parity(drain_groups(odd_groups, downward, downs), drain_groups(even_groups, upward, ups))
-    for copy in (wh_copy, wc_copy, conv_copy, mate_head):
-        copy.wait_send()
+    mate_copy(wc, wc, 0).wait_send()
+    conv_copy.wait_send()
+    mate_head.wait_send()
     for step in steps:
-        for g in range(GROUPS):
-            wf_copy(step, g).wait_send()
+        wf_copy(step, tuple(range(GROUPS))).wait_send()
         cy_copy(step).wait_send()
-        for ob in range(2):
-            ha_copy(step, ob).wait_send()
+        ha_sent(step).wait_send()
 
 
 def shards(n_sp, n_tp, *args):
@@ -529,16 +593,15 @@
     dma = pltpu.SemaphoreType.DMA
     hbm = pl.BlockSpec(memory_space=pltpu.HBM)
     scratch = [
-        pltpu.VMEM(gate.shape, BF16),
-        pltpu.VMEM(mix.shape, BF16),
-        pltpu.VMEM(inp.shape, BF16),
+        pltpu.VMEM((2, rows, lanes), BF16),
+        pltpu.VMEM((2, rows, lanes), BF16),
         pltpu.VMEM(taps.shape, BF16),
         pltpu.VMEM((1, gain.shape[0]), F32),
-        pltpu.VMEM(q.shape, BF16),
         pltpu.VMEM((levels, 2, rows, lanes), BF16),
         pltpu.VMEM((levels, 2, rows, lanes), BF16),
-        pltpu.VMEM((2, 16, mix.shape[1]), BF16),
-        pltpu.VMEM((rows + 8, mix.shape[1]), F32),
+        pltpu.VMEM((2, 16, lanes), BF16),
+        pltpu.VMEM((2, 16, lanes), BF16),
+        pltpu.VMEM((rows + 8, lanes), F32),
         pltpu.VMEM((rows, 2 * lanes), BF16),
         pltpu.VMEM((2 * depth, width), BF16),
         pltpu.VMEM((n_tp * depth, width), BF16),
@@ -549,20 +612,25 @@
         pltpu.VMEM((chunk, n_tp * depth), BF16),
         pltpu.VMEM((2, rows, depth), F32),
         pltpu.VMEM((2, rows, 2 * depth), F32),
-        dma((2 * PIECES + 8,)),
+        dma((7,)),
         dma((2,)),
         dma((2,)),
-        dma((levels, PIECES)),
-        dma((levels, PIECES)),
-        dma((levels, PIECES)),
-        dma((levels, PIECES)),
-        dma((4,)),
+        dma((max(levels - 1, 1),)),
+        dma((max(levels - 1, 1), PIECES)),
+        dma((levels,)),
+        dma((levels,)),
+        dma((1,)),
+        dma((1,)),
+        dma((PIECES // 2,)),
+        dma((3,)),
         dma((4,)),
         dma((outer - 1,)),
         dma((outer - 1,)),
-        dma((outer - 1, 2)),
-        dma((outer - 1, 2)),
-    ] + [dma((outer - 1, GROUPS))] * 6
+        dma((outer - 1,)),
+        dma((outer - 1,)),
+        dma((outer - 1,)),
+        dma((outer - 1, GROUPS - min(len(UPWARD), len(DOWNWARD)) if levels % 2 == 0 else GROUPS)),
+    ] + [dma((outer - 1,))] * 4
     return pl.pallas_call(
         functools.partial(kernel, n_sp, n_tp),
         out_shape=pltpu.VMEM((chunk, width), BF16),

time: 22.8 us -> 20.8 us (0.912)
  Pallas kernels: 21.3 us -> 19.3 us
    pallas_call x1, Pallas kernels: 21.3 us -> 19.3 us  [shards(): pl.pallas_call(functools.partial(kernel, n_sp, n_tp), out_shape=pltpu.VME...]
where the time goes in v3:
time: 20.8 us; the launch traced here: 20.7 us
  Pallas kernels  19.3 us (93%)
  local copies, waits for them, and re-layouts  0.71 us (3%)
  between operations  0.66 us (3%)
    pallas_call x1, Pallas kernels, shards(): pl.pallas_call(functools.partial(kernel, n_sp, n_tp), out_shape=pltpu.VME...  19.3 us
    unnamed x1, local copies, waits for them, and re-layouts  0.71 us

profile of v3, /device:TPU:25, one launch (start us, length us, event | category | flops | bytes accessed | tf_op | source)
XLA Modules:
  0.0 20.7 jit_solution(15440500192377459743)
XLA Ops:
  0.7 19.3 %shard_map.109 = bf16[64,2048]{1,0:T(8,128)(2,1)S(1)} custom-call(bf16[256,128]{1,0:T(8,128)(2,1)} %gate_h.1, bf16[256,128]{1,0:T(8,128)(2,1)} %mix_h.1, bf16[256,128]{1,0:T(8,128)(2,1)} %inp_h.1, bf16[3,128]{1,0:T(4,128)(2,1)} %taps_h.1, bf16[256,128]{1,0:T(8,128)(2,1)} %q_h.1, bf16[256,128]{1,0:T(8,128)(2,1)} %k_h.1, bf16[256,128]{1,0:T(8,128)(2,1)} %v_h.1, ...), custom_call_target="tpu_custom_call" | custom-call | tf_op jit(solution)/shard_map/pallas_call | solution.py:634
  19.9 0.7 %copy.13 = bf16[64,2048]{1,0:T(8,128)(2,1)} copy(bf16[64,2048]{1,0:T(8,128)(2,1)S(1)} %shard_map.109) | data formatting | bytes 524288
